TPU v7x, 32 devices: a whole 2x2x4 slice. The times are simulated.
32 devices in a mesh: grp: 2 (over y), sp: 4 (over z), tp: 4 (over x, core).
Axes of the slice: x: 2, y: 2, z: 4, core: 2. Of those that a mesh axis runs over, the one named last changes fastest.
Arguments:
- conv_value: bfloat16 [4096, 1024], P(('grp', 'sp'), 'tp'), parts along dimension 0, may hold values from -6 to 6
- conv_gate: bfloat16 [4096, 1024], P(('grp', 'sp'), 'tp'), parts along dimension 0, may hold values from -6 to 6
- kernel: bfloat16 [31, 1024], P(None, 'tp'), may hold values from -4 to 4
- conv_bias: float32 [1024], P('tp'), may hold values from -3 to 3
- ln_gain: float32 [1024], P('tp'), may hold values from 0.1 to 1.9
- ln_bias: float32 [1024], P('tp'), may hold values from -3 to 3
- out_gain: float32 [1024], P('tp'), may hold values from 0.1 to 1.9
- out_weight: bfloat16 [1024, 2048], replicated, may hold values from -0.1875 to 0.1875
- residual: bfloat16 [4096, 2048], P(('grp', 'sp', 'tp')), parts along dimension 0, may hold values from -6 to 6
- moe_gain: float32 [2048], replicated, may hold values from 0.1 to 1.9
- expert_ids: int32 [4096, 2], P(('grp', 'sp', 'tp')), parts along dimension 0, may hold values from 0 to 15, as said below
- expert_weights: float32 [4096, 2], P(('grp', 'sp', 'tp')), parts along dimension 0, may hold values from 0.1 to 0.7
- w_gate: bfloat16 [16, 2048, 512], P(('sp', 'tp')), may hold values from -0.125 to 0.125
- w_up: bfloat16 [16, 2048, 512], P(('sp', 'tp')), may hold values from -0.125 to 0.125
- w_down: bfloat16 [16, 512, 2048], P(('sp', 'tp')), may hold values from -0.25 to 0.25
Outputs:
- layer_out: bfloat16 [4096, 2048], P(('grp', 'sp', 'tp')), parts along dimension 0
There are 2 independent parts, one for each index of `grp`. A program takes and returns all parts, laid end to end along the dimension named above; an argument that names none is the same for every part. Nothing has to cross between parts.
Inputs may be any that keep to these rules, and one draw needn't show every extreme that they name: `expert_ids`: each row names two different experts of one group (group = expert number // 4). Among the 128 rows of one device (aligned blocks of 128 rows) no expert is named more than 32 times, and in every such block some expert is named exactly 32 times.
All inputs are finite; a program needn't handle non-finite values.
Results may differ from a plain program's by a relative error of at most 0.0095.
Values may be sent and summed in bfloat16 or wider, within the bound.
A program may use at most 64 MiB of HBM per device.

v0:
```python
import jax
import jax.numpy as jnp
from jax import lax
from jax.sharding import PartitionSpec as P

EPSILON = 1e-06


def passed_along(block, axis, distance):
    devices = range(lax.axis_size(axis))
    route = [(i - distance, i) for i in devices if i - distance in devices]
    return lax.ppermute(block, axis, route)


def per_device(
    conv_value,
    conv_gate,
    kernel,
    conv_bias,
    ln_gain,
    ln_bias,
    out_gain,
    out_weight,
    residual,
    moe_gain,
    expert_ids,
    expert_weights,
    w_gate,
    w_up,
    w_down,
):
    tok_rows, channels = conv_value.shape
    reach_rows = kernel.shape[0] - 1
    full_channels = channels * lax.axis_size("tp")
    gated = (conv_value.astype(jnp.float32) * jax.nn.sigmoid(conv_gate.astype(jnp.float32))).astype(
        jnp.bfloat16
    )
    before = passed_along(gated[tok_rows - reach_rows :], "sp", 1)
    padded = jnp.concatenate([before, gated], axis=0)
    convolved = jnp.zeros((tok_rows, channels), jnp.float32) + conv_bias
    for offset in range(reach_rows + 1):
        convolved = convolved + padded[offset : offset + tok_rows].astype(jnp.float32) * kernel[
            offset
        ].astype(jnp.float32)
    totals = lax.psum((jnp.sum(convolved, axis=1), jnp.sum(convolved * convolved, axis=1)), "tp")
    average = (totals[0] / full_channels)[:, None]
    spread = (totals[1] / full_channels)[:, None] - average * average
    swished = jax.nn.silu((convolved - average) * lax.rsqrt(spread + EPSILON) * ln_gain + ln_bias)
    energy = lax.psum(jnp.sum(swished * swished, axis=1), "tp")
    branch = (swished * lax.rsqrt(energy / full_channels + EPSILON)[:, None] * out_gain).astype(
        jnp.bfloat16
    )
    row_count = tok_rows // lax.axis_size("tp")
    regrouped = lax.all_to_all(branch, "tp", split_axis=0, concat_axis=1, tiled=True)
    projected = jnp.dot(regrouped, out_weight, preferred_element_type=jnp.float32)
    hidden = (residual.astype(jnp.float32) + projected).astype(jnp.bfloat16)
    widened = hidden.astype(jnp.float32)
    normed = (
        widened * lax.rsqrt(jnp.mean(widened * widened, axis=1, keepdims=True) + EPSILON) * moe_gain
    ).astype(jnp.bfloat16)
    width = normed.shape[1]
    experts = lax.axis_size("sp") * lax.axis_size("tp")
    capacity = 2 * row_count // min(row_count, experts // 2)
    flat_ids = expert_ids.reshape(-1)
    onehot = (flat_ids[:, None] == jnp.arange(experts, dtype=jnp.int32)[None, :]).astype(jnp.int32)
    slot_rank = jnp.sum((jnp.cumsum(onehot, axis=0) - 1) * onehot, axis=1)
    position = flat_ids * capacity + slot_rank
    outgoing = (
        jnp.zeros((experts * capacity, width), jnp.bfloat16)
        .at[position]
        .set(jnp.repeat(normed, 2, axis=0))
    )
    outgoing = outgoing.reshape(experts, capacity, width)
    arriving = lax.all_to_all(outgoing, ("sp", "tp"), split_axis=0, concat_axis=0, tiled=True)
    flattened = arriving.reshape(-1, width)
    gate_part = jnp.dot(flattened, w_gate[0], preferred_element_type=jnp.float32)
    up_part = jnp.dot(flattened, w_up[0], preferred_element_type=jnp.float32)
    active = (jax.nn.silu(gate_part) * up_part).astype(jnp.bfloat16)
    result = jnp.dot(active, w_down[0], preferred_element_type=jnp.float32).astype(jnp.bfloat16)
    produced = result.reshape(arriving.shape)
    returned = lax.all_to_all(produced, ("sp", "tp"), split_axis=0, concat_axis=0, tiled=True)
    returned = returned.reshape(experts * capacity, width)
    picked = returned[position].reshape(row_count, 2, width)
    combined = jnp.sum(picked.astype(jnp.float32) * expert_weights[:, :, None], axis=1)
    return (widened + combined).astype(jnp.bfloat16)


def solution(mesh):
    in_specs = (
        P(("grp", "sp"), "tp"),
        P(("grp", "sp"), "tp"),
        P(None, "tp"),
        P("tp"),
        P("tp"),
        P("tp"),
        P("tp"),
        P(),
        P(("grp", "sp", "tp"), None),
        P(),
        P(("grp", "sp", "tp"), None),
        P(("grp", "sp", "tp"), None),
        P(("sp", "tp"), None, None),
        P(("sp", "tp"), None, None),
        P(("sp", "tp"), None, None),
    )
    out_specs = P(("grp", "sp", "tp"), None)
    return jax.shard_map(
        per_device, mesh=mesh, in_specs=in_specs, out_specs=out_specs, check_vma=False
    )
```

profile of v0, /device:TPU:13, one launch (start us, length us, event | category | flops | bytes accessed | tf_op | source)
XLA Modules:
  0.0 175.2 jit_solution(14882649064990953928)
XLA Ops:
  0.0 1.3 multiply_convert_fusion.2
  1.4 3.2 %collective-permute-start = (bf16[30,256]{1,0:T(8,128)(2,1)S(1)}, bf16[30,256]{1,0:T(8,128)(2,1)S(1)}, u32[]{:S(2)}, u32[]{:S(2)}) collective-permute-start(bf16[30,256]{1,0:T(8,128)(2,1)S(1)} %slice.258), channel_id=1, source_target_pairs={{0,4},{4,8},{8,12},{1,5},{5,9},{9,13},{2,6},{6,10},{10,14},{3,7},{... | collective-permute-start | bytes 46088 | tf_op jit(solution)/shard_map/ppermute | solution.py:12
  4.6 1.0 slice_convert_fusion.30
  5.6 1.0 slice_convert_fusion.29
  9.5 3.2 %fusion.51 = (f32[512]{0:T(512)S(1)}, f32[512]{0:T(512)S(1)}, f32[512,256]{1,0:T(8,128)S(1)}) fusion(f32[256]{0:T(256)S(1)} %bitcast.109, bf16[512,256]{1,0:T(8,128)(2,1)S(1)} %multiply_convert_fusion.2, f32[256]{0:T(256)S(1)} %bitcast.110, bf16[30,256]{1,0:T(8,128)(2,1)S(1)} %collective-permute-done, f32[256]{0:T(256)S(1)} %bitcast.81, ...), kind=kLoop, calls=%fused_computation.137 | loop fusion | flops 24378368 | bytes 838656 | tf_op jit(solution)/shard_map/reduce_sum | solution.py:45
  12.7 6.0 %all-reduce = (f32[512]{0:T(512)S(1)}, f32[512]{0:T(512)S(1)}) all-reduce(f32[512]{0:T(512)S(1)} %get-tuple-element.6, f32[512]{0:T(512)S(1)} %get-tuple-element.5), channel_id=1, replica_groups=mesh['grp'=2,'sp'=4,'tp'=4] {'tp'}, use_global_device_ids=true, to_apply=%region_3.0 | all-reduce | flops 1024 | bytes 8192 | tf_op jit(solution)/shard_map/psum | solution.py:45
  19.1 6.3 %psum.23 = f32[512]{0:T(512)S(1)} all-reduce(f32[512]{0:T(512)S(1)} %get-tuple-element.9), channel_id=1, replica_groups=mesh['grp'=2,'sp'=4,'tp'=4] {'tp'}, use_global_device_ids=true, to_apply=%region_5.6 | all-reduce | flops 512 | bytes 4096 | tf_op jit(solution)/shard_map/psum | solution.py:49
  25.4 0.8 multiply_convert_fusion.1
  26.3 4.3 %all-to-all-start = ((bf16[4,128,256]{2,1,0:T(8,128)(2,1)}), bf16[4,128,256]{2,1,0:T(8,128)(2,1)S(1)}, u32[]{:S(2)}, u32[]{:S(2)}) async-start(bf16[4,128,256]{2,1,0:T(8,128)(2,1)} %bitcast.31), calls=%async_computation | async-start | bytes 524288 | tf_op jit(solution)/shard_map/all_to_all | solution.py:54
  30.6 5.0 %all-to-all-done = bf16[4,128,256]{2,1,0:T(8,128)(2,1)S(1)} async-done(((bf16[4,128,256]{2,1,0:T(8,128)(2,1)}), bf16[4,128,256]{2,1,0:T(8,128)(2,1)S(1)}, u32[]{:S(2)}, u32[]{:S(2)}) %all-to-all-start) | async-done | bytes 262176 | tf_op jit(solution)/shard_map/all_to_all | solution.py:54
  35.8 3.1 %multiply_reduce_fusion.1 = (f32[128]{0:T(128)S(1)}, f32[128,2048]{1,0:T(8,128)S(1)}) fusion(bf16[128,1024]{0,1:T(8,128)(2,1)S(1)} %bitcast.78, bf16[1024,2048]{1,0:T(8,128)(2,1)} %param.22, bf16[128,2048]{1,0:T(8,128)(2,1)} %param.23), kind=kOutput, calls=%fused_computation.45 | convolution fusion | flops 538443648 | bytes 6029824 | tf_op jit(solution)/shard_map/dot_general | solution.py:55
  39.1 1.6 broadcast_in_dim.5
  40.8 2.3 %reshape.140 = bf16[256,2048]{1,0:T(8,128)(2,1)} reshape(bf16[128,2,2048]{2,1,0:T(2,128)(2,1)} %broadcast_in_dim.5) | data formatting | bytes 2097152 | tf_op jit(solution)/shard_map/reshape | solution.py:71
  43.0 4.4 %scatter_custom_fusion = bf16[512,2048]{1,0:T(8,128)(2,1)} fusion(s32[256]{0:T(256)S(1)} %bitcast.112, bf16[256,2048]{1,0:T(8,128)(2,1)} %reshape.140, bf16[]{:T(256)} %constant.15.clone.1), kind=kCustom, calls=%fused_computation.46 | custom fusion | bytes 2097664 | tf_op jit(solution)/shard_map/scatter | solution.py:71
  47.4 52.9 %all_to_all.29 = bf16[16,32,2048]{2,1,0:T(8,128)(2,1)S(1)} all-to-all(bf16[16,32,2048]{2,1,0:T(8,128)(2,1)} %bitcast.74), channel_id=1, replica_groups=mesh['grp'=2,'sp'=4,'tp'=4] {'sp','tp'}, dimensions={0} | all-to-all | bytes 4194304 | tf_op jit(solution)/shard_map/all_to_all | solution.py:74
  100.3 1.3 copy-done.1
  101.6 2.2 %fusion.5 = f32[512,512]{1,0:T(8,128)} fusion(bf16[512,2048]{1,0:T(8,128)(2,1)S(1)} %bitcast.76, bf16[1,2048,512]{2,1,0:T(8,128)(2,1)S(1)} %copy-done.7), kind=kOutput, calls=%fused_computation.38 | convolution fusion | flops 1073741824 | bytes 5242880 | tf_op jit(solution)/shard_map/dot_general | solution.py:76
  103.8 6.3 %convolution_convert_fusion = bf16[512,2048]{1,0:T(8,128)(2,1)} fusion(bf16[1,512,2048]{2,1,0:T(8,128)(2,1)S(1)} %copy-done, bf16[512,2048]{1,0:T(8,128)(2,1)} %bitcast.77, bf16[1,2048,512]{2,1,0:T(8,128)(2,1)} %param.28, f32[512,512]{1,0:T(8,128)} %fusion.5), kind=kOutput, calls=%fused_computation.31 | convolution fusion | flops 2150105088 | bytes 9437184 | tf_op jit(solution)/shard_map/dot_general | solution.py:79
  110.1 4.7 %all-to-all-start.2 = ((bf16[16,32,2048]{2,1,0:T(8,128)(2,1)}), bf16[16,32,2048]{2,1,0:T(8,128)(2,1)}, u32[]{:S(2)}, u32[]{:S(2)}) async-start(bf16[16,32,2048]{2,1,0:T(8,128)(2,1)} %bitcast.75), calls=%async_computation.2 | async-start | bytes 4194304 | tf_op jit(solution)/shard_map/all_to_all | solution.py:81
  114.9 46.0 %all-to-all-done.2 = bf16[16,32,2048]{2,1,0:T(8,128)(2,1)} async-done(((bf16[16,32,2048]{2,1,0:T(8,128)(2,1)}), bf16[16,32,2048]{2,1,0:T(8,128)(2,1)}, u32[]{:S(2)}, u32[]{:S(2)}) %all-to-all-start.2) | async-done | bytes 2097184 | tf_op jit(solution)/shard_map/all_to_all | solution.py:81
  160.9 5.2 %gather_fusion = bf16[256,2048]{1,0:T(8,128)(2,1)} fusion(bf16[512,2048]{1,0:T(8,128)(2,1)} %bitcast.43, s32[1024]{0:T(1024)S(1)} %pad_clamp_fusion), kind=kCustom, calls=%fused_computation | custom fusion | bytes 2098176 | tf_op jit(solution)/shard_map/gather | solution.py:83
  166.1 3.4 %reshape.127 = f32[128,2,2048]{2,1,0:T(2,128)} reshape(bf16[256,2048]{1,0:T(8,128)(2,1)} %gather_fusion) | data formatting | bytes 3145728 | tf_op jit(solution)/shard_map/convert_element_type | solution.py:84
  169.5 4.8 %multiply_reduce_fusion = f32[128,2048]{1,0:T(8,128)S(1)} fusion(f32[128,2,2048]{2,1,0:T(2,128)} %reshape.127, f32[128,2]{1,0:T(8,128)S(1)} %copy.27), kind=kLoop, calls=%fused_computation.40 | loop fusion | flops 786432 | bytes 3146752 | tf_op jit(solution)/shard_map/reduce_sum | solution.py:84
  174.3 0.9 add_convert_fusion
  (38 shorter events, 3.8 us)
Async XLA Ops:
  0.0 103.8 %copy-start = (bf16[1,512,2048]{2,1,0:T(8,128)(2,1)S(1)}, bf16[1,512,2048]{2,1,0:T(8,128)(2,1)}, u32[]{:S(2)}) copy-start(bf16[1,512,2048]{2,1,0:T(8,128)(2,1)} %param.29) | copy-start | bytes 6291460
  0.0 18.7 %copy-start.6 = (f32[256]{0:T(256)S(1)}, f32[256]{0:T(256)}, u32[]{:S(2)}) copy-start(f32[256]{0:T(256)} %param.19) | copy-start | bytes 3076
  0.0 18.7 %copy-start.5 = (f32[256]{0:T(256)S(1)}, f32[256]{0:T(256)}, u32[]{:S(2)}) copy-start(f32[256]{0:T(256)} %param.20) | copy-start | bytes 3076
  0.0 25.4 %copy-start.3 = (f32[256]{0:T(256)S(1)}, f32[256]{0:T(256)}, u32[]{:S(2)}) copy-start(f32[256]{0:T(256)} %param.21) | copy-start | bytes 3076
  1.4 8.1 %collective-permute-start = (bf16[30,256]{1,0:T(8,128)(2,1)S(1)}, bf16[30,256]{1,0:T(8,128)(2,1)S(1)}, u32[]{:S(2)}, u32[]{:S(2)}) collective-permute-start(bf16[30,256]{1,0:T(8,128)(2,1)S(1)} %slice.258), channel_id=1, source_target_pairs={{0,4},{4,8},{8,12},{1,5},{5,9},{9,13},{2,6},{6,10},{10,14},{3,7},{... | collective-permute-start | bytes 46088 | tf_op jit(solution)/shard_map/ppermute | solution.py:12
  26.3 9.4 %all-to-all-start = ((bf16[4,128,256]{2,1,0:T(8,128)(2,1)}), bf16[4,128,256]{2,1,0:T(8,128)(2,1)S(1)}, u32[]{:S(2)}, u32[]{:S(2)}) async-start(bf16[4,128,256]{2,1,0:T(8,128)(2,1)} %bitcast.31), calls=%async_computation | async-start | bytes 524288 | tf_op jit(solution)/shard_map/all_to_all | solution.py:54
  35.8 3.2 %copy-start.2 = (f32[2048]{0:T(1024)S(1)}, f32[2048]{0:T(1024)}, u32[]{:S(2)}) copy-start(f32[2048]{0:T(1024)} %param.24) | copy-start | bytes 24580
  47.4 54.2 %copy-start.7 = (bf16[1,2048,512]{2,1,0:T(8,128)(2,1)S(1)}, bf16[1,2048,512]{2,1,0:T(8,128)(2,1)}, u32[]{:S(2)}) copy-start(bf16[1,2048,512]{2,1,0:T(8,128)(2,1)} %param.27) | copy-start | bytes 6291460
  100.3 1.3 copy-start.1
  110.1 4.7 %copy-start.4 = (f32[128,2]{0,1:T(2,128)S(1)}, f32[128,2]{0,1:T(2,128)}, u32[]{:S(2)}) copy-start(f32[128,2]{0,1:T(2,128)} %param.26) | copy-start | bytes 3076
  110.1 50.8 %all-to-all-start.2 = ((bf16[16,32,2048]{2,1,0:T(8,128)(2,1)}), bf16[16,32,2048]{2,1,0:T(8,128)(2,1)}, u32[]{:S(2)}, u32[]{:S(2)}) async-start(bf16[16,32,2048]{2,1,0:T(8,128)(2,1)} %bitcast.75), calls=%async_computation.2 | async-start | bytes 4194304 | tf_op jit(solution)/shard_map/all_to_all | solution.py:81
where the time goes:
time: 177 us; the launch traced here: 175 us
  blocking collectives  65.1 us (37%)
  waiting for transfers between devices  51 us (29%)
  local copies, waits for them, and re-layouts  20 us (11%)
  other arithmetic  15.1 us (9%)
  starting transfers between devices  12.2 us (7%)
  matrix products  11.6 us (7%)
    all_to_all x1, blocking collectives, per_device(): lax.all_to_all(outgoing, ('sp', 'tp'), split_axis=0, concat_axis=0, tiled...  52.9 us
    all_to_all x1, waiting for transfers between devices, per_device(): lax.all_to_all(produced, ('sp', 'tp'), split_axis=0, concat_axis=0, tiled...  46 us
    psum x1, blocking collectives, per_device(): energy = lax.psum(jnp.sum(swished * swished, axis=1), 'tp')  6.31 us
    dot_general x1, matrix products, per_device(): jnp.dot(active, w_down[0], preferred_element_type=jnp.float32)  6.27 us
    psum x1, blocking collectives, per_device(): lax.psum((jnp.sum(convolved, axis=1), jnp.sum(convolved * convolved, axis...  5.97 us
    gather x1, local copies, waits for them, and re-layouts, per_device(): picked = returned[position].reshape(row_count, 2, width)  5.2 us
    all_to_all x1, waiting for transfers between devices, per_device(): lax.all_to_all(branch, 'tp', split_axis=0, concat_axis=1, tiled=True)  5.04 us
    reduce_sum x1, other arithmetic, per_device(): jnp.sum(picked.astype(jnp.float32) * expert_weights[:, :, None], axis=1)  4.81 us
  transfers between devices with their start and end apart: 3, of which 2 were waited for; matrix products, arithmetic and copies ran while one was open for 3% of the time, Pallas kernels for 0%

commit v1 on v0

--- a/solution.py
+++ b/solution.py
@@ -1,9 +1,238 @@
 import jax
 import jax.numpy as jnp
 from jax import lax
+from jax.experimental import pallas as pl
+from jax.experimental.pallas import tpu as pltpu
 from jax.sharding import PartitionSpec as P
 
 EPSILON = 1e-06
+GROUPS = 4
+LANES = 128
+SUBLANES = 8
+MESH = pl.DeviceIdType.MESH
+
+
+def flipped(index, mask, size):
+    total, bit = 0, 1
+    while bit < size:
+        total = total + ((index // bit + mask // bit) % 2) * bit
+        bit *= 2
+    return total
+
+
+def routed_kernel(
+    send, meta, gate_hbm, up_hbm, down_hbm, out,
+    w_gate, w_up, w_down, rows, weights, own, half_out, half_in, cross_out, cross_in, final, act,
+    load_sem, meta_s, meta_r, z_s, z_r, pair_s, pair_r, x_s, x_r, via_s, via_r,
+    half_s, half_r, cross_s, cross_r, back_s, back_r,
+):
+    spn, tpn, cap, width = rows.shape
+    me_z, me_t = lax.axis_index("sp"), lax.axis_index("tp")
+    pair, across = flipped(me_t, 1, tpn), flipped(me_t, 2, tpn)
+    hidden = w_gate.shape[1]
+
+    def to(z, t):
+        return {"sp": z, "tp": t}
+
+    def copy(src, dst, s, r, z, t):
+        return pltpu.make_async_remote_copy(
+            src_ref=src, dst_ref=dst, send_sem=s, recv_sem=r, device_id=to(z, t), device_id_type=MESH
+        )
+
+    loads = [
+        pltpu.make_async_copy(a, b, load_sem.at[i])
+        for i, (a, b) in enumerate(((gate_hbm, w_gate), (up_hbm, w_up), (down_hbm, w_down)))
+    ]
+    for load in loads:
+        load.start()
+
+    peers = [(k, r) for k in range(spn) for r in range(tpn) if k or r]
+    barrier = pltpu.get_barrier_semaphore()
+    for k, r in peers:
+        pl.semaphore_signal(
+            barrier, inc=1, device_id=to(flipped(me_z, k, spn), flipped(me_t, r, tpn)), device_id_type=MESH
+        )
+    pl.semaphore_wait(barrier, len(peers))
+
+    def z_copy(k):
+        return copy(send.at[k], rows.at[k, 0], z_s.at[k], z_r.at[k], flipped(me_z, k, spn), me_t)
+
+    def meta_copy(k, r):
+        return copy(
+            meta.at[k], weights.at[k, r], meta_s.at[k, r], meta_r.at[k, r],
+            flipped(me_z, k, spn), flipped(me_t, r, tpn),
+        )
+
+    def pair_copy(k):
+        return copy(rows.at[k, 0], rows.at[k, 1], pair_s.at[k], pair_r.at[k], me_z, pair)
+
+    def x_copy(k):
+        return copy(rows.at[k, 0], rows.at[k, 2], x_s.at[k], x_r.at[k], me_z, across)
+
+    def via_copy(k):
+        return copy(rows.at[k, 2], rows.at[k, 3], via_s.at[k], via_r.at[k], me_z, pair)
+
+    def half_copy(k):
+        return copy(half_out.at[k], half_in.at[k], half_s.at[k], half_r.at[k], me_z, pair)
+
+    def cross_copy(k):
+        return copy(cross_out.at[k], cross_in.at[k], cross_s.at[k], cross_r.at[k], me_z, across)
+
+    def back_copy(k):
+        return copy(final.at[k], out.at[k], back_s.at[k], back_r.at[k], flipped(me_z, k, spn), me_t)
+
+    for k, r in peers:
+        meta_copy(k, r).start()
+    for k in range(1, spn):
+        z_copy(k).start()
+    weights[0, 0] = meta[0]
+    rows[0, 0] = send[0]
+    x_copy(0).start()
+    pair_copy(0).start()
+    for k, r in peers:
+        meta_copy(k, r).wait_recv()
+    for load in loads:
+        load.wait()
+
+    tile = min(hidden, 512)
+    diagonal = (
+        lax.broadcasted_iota(jnp.int32, (cap, LANES), 0) == lax.broadcasted_iota(jnp.int32, (cap, LANES), 1)
+    )
+
+    def compute(k):
+        x = rows[k].reshape(tpn * cap, width)
+        for c in range(0, hidden, 256):
+            g = jnp.dot(x, w_gate[:, c : c + 256], preferred_element_type=jnp.float32)
+            u = jnp.dot(x, w_up[:, c : c + 256], preferred_element_type=jnp.float32)
+            act[:, c : c + 256] = (g / (1.0 + jnp.exp(-g)) * u).astype(jnp.bfloat16)
+        a = act[...]
+        scales = [
+            jnp.sum(jnp.where(diagonal, weights[k, r, pl.ds(me_t, 1), :], 0.0), axis=1, keepdims=True)
+            for r in range(tpn)
+        ]
+
+        def column(c, carry):
+            cols = pl.ds(pl.multiple_of(c * tile, tile), tile)
+            res = jnp.dot(a, w_down[:, cols], preferred_element_type=jnp.float32).astype(jnp.bfloat16)
+            res = res.astype(jnp.float32)
+            parts = [res[r * cap : (r + 1) * cap] * scales[r] for r in range(tpn)]
+            half_out[k, 0, :, cols] = parts[1].astype(jnp.bfloat16)
+            half_out[k, 1, :, cols] = parts[3].astype(jnp.bfloat16)
+            own[k, 0, :, cols] = parts[0]
+            own[k, 1, :, cols] = parts[2]
+            return carry
+
+        lax.fori_loop(0, width // tile, column, 0)
+
+    def step(i, carry):
+        @pl.when(i + 1 < spn)
+        def _():
+            k = i + 1
+            z_copy(k).wait_recv()
+            x_copy(k).start()
+            pair_copy(k).start()
+
+        @pl.when(i < spn)
+        def _():
+            x_copy(i).wait_recv()
+            via_copy(i).start()
+            pair_copy(i).wait_recv()
+            via_copy(i).wait_recv()
+            compute(i)
+            half_copy(i).start()
+
+        @pl.when((i >= 1) & (i <= spn))
+        def _():
+            k = i - 1
+            half_copy(k).wait_recv()
+            cross_out[k] = (own[k, 1] + half_in[k, 1].astype(jnp.float32)).astype(jnp.bfloat16)
+            cross_copy(k).start()
+
+        @pl.when(i >= 2)
+        def _():
+            k = i - 2
+            cross_copy(k).wait_recv()
+            final[k] = (
+                own[k, 0] + half_in[k, 0].astype(jnp.float32) + cross_in[k].astype(jnp.float32)
+            ).astype(jnp.bfloat16)
+
+            @pl.when(k >= 1)
+            def _():
+                back_copy(k).start()
+
+        return carry
+
+    lax.fori_loop(0, spn + 2, step, 0)
+    out[0] = final[0]
+    for k, r in peers:
+        meta_copy(k, r).wait_send()
+    for k in range(spn):
+        for make in (x_copy, pair_copy, via_copy, half_copy, cross_copy):
+            make(k).wait_send()
+    for k in range(1, spn):
+        z_copy(k).wait_send()
+        back_copy(k).wait_send()
+        back_copy(k).wait_recv()
+
+
+def routed_experts(send, meta, w_gate, w_up, w_down):
+    spn, cap, width = send.shape
+    tpn = lax.axis_size("tp")
+    hidden = w_gate.shape[1]
+    bf, f32, dma = jnp.bfloat16, jnp.float32, pltpu.SemaphoreType.DMA
+    vmem = pl.BlockSpec(memory_space=pltpu.VMEM)
+    hbm = pl.BlockSpec(memory_space=pl.ANY)
+    return pl.pallas_call(
+        routed_kernel,
+        out_shape=jax.ShapeDtypeStruct((spn, cap, width), bf),
+        in_specs=[vmem, vmem, hbm, hbm, hbm],
+        out_specs=vmem,
+        scratch_shapes=[
+            pltpu.VMEM(w_gate.shape, bf),
+            pltpu.VMEM(w_up.shape, bf),
+            pltpu.VMEM(w_down.shape, bf),
+            pltpu.VMEM((spn, tpn, cap, width), bf),
+            pltpu.VMEM((spn, tpn, SUBLANES, LANES), f32),
+            pltpu.VMEM((spn, 2, cap, width), f32),
+            pltpu.VMEM((spn, 2, cap, width), bf),
+            pltpu.VMEM((spn, 2, cap, width), bf),
+            pltpu.VMEM((spn, cap, width), bf),
+            pltpu.VMEM((spn, cap, width), bf),
+            pltpu.VMEM((spn, cap, width), bf),
+            pltpu.VMEM((tpn * cap, hidden), bf),
+            dma((3,)),
+            dma((spn, tpn)),
+            dma((spn, tpn)),
+        ]
+        + [dma((spn,))] * 14,
+        compiler_params=pltpu.CompilerParams(collective_id=0, has_side_effects=True),
+    )(send, meta, w_gate, w_up, w_down)
+
+
+def route_by_group(normed, widened, expert_ids, expert_weights, w_gate, w_up, w_down):
+    spn, tpn = lax.axis_size("sp"), lax.axis_size("tp")
+    row_count, width = normed.shape
+    capacity = 2 * row_count // min(row_count, spn * tpn // 2)
+    cap = tpn * capacity // 2
+    group = expert_ids[:, 0] // tpn
+    place = jnp.arange(row_count, dtype=jnp.int32)
+    earlier = (group[None, :] == group[:, None]) & (place[None, :] < place[:, None])
+    rank = jnp.sum(earlier.astype(jnp.int32), axis=1)
+    slot = flipped(group, lax.axis_index("sp"), spn) * cap + rank
+    chosen = jnp.arange(spn * cap, dtype=jnp.int32)[:, None] == slot[None, :]
+    pick = chosen.astype(jnp.bfloat16)
+    send = jnp.dot(pick, normed, preferred_element_type=jnp.float32).astype(jnp.bfloat16)
+    member = (expert_ids[:, :, None] % tpn) == jnp.arange(SUBLANES, dtype=jnp.int32)[None, None, :]
+    by_expert = jnp.sum(jnp.where(member, expert_weights[:, :, None], 0.0), axis=1)
+    meta = jnp.sum(
+        jnp.where(chosen[None, :, :], by_expert.T[:, None, :], 0.0), axis=2
+    ).reshape(SUBLANES, spn, cap)
+    meta = jnp.pad(meta.transpose(1, 0, 2), ((0, 0), (0, 0), (0, LANES - cap)))
+    back = routed_experts(send.reshape(spn, cap, width), meta, w_gate[0], w_up[0], w_down[0])
+    combined = lax.dot_general(
+        pick, back.reshape(spn * cap, width), (((0,), (0,)), ((), ())), preferred_element_type=jnp.float32
+    )
+    return (widened + combined).astype(jnp.bfloat16)
 
 
 def passed_along(block, axis, distance):
@@ -60,6 +289,10 @@
     ).astype(jnp.bfloat16)
     width = normed.shape[1]
     experts = lax.axis_size("sp") * lax.axis_size("tp")
+    if experts // GROUPS == lax.axis_size("tp") and lax.axis_size("tp") == 4:
+        return route_by_group(
+            normed, widened, expert_ids, expert_weights, w_gate, w_up, w_down
+        )
     capacity = 2 * row_count // min(row_count, experts // 2)
     flat_ids = expert_ids.reshape(-1)
     onehot = (flat_ids[:, None] == jnp.arange(experts, dtype=jnp.int32)[None, :]).astype(jnp.int32)

time: 177 us -> 119 us (0.67)
  Pallas kernels: 0 us -> 74.7 us
  blocking collectives: 65.1 us -> 12.3 us
  waiting for transfers between devices: 51 us -> 3.99 us
  local copies, waits for them, and re-layouts: 20 us -> 0.88 us
  matrix products: 11.6 us -> 6.88 us
  starting transfers between devices: 12.2 us -> 7.54 us
  other arithmetic: 15.1 us -> 12.4 us
    pallas_call x0 -> x1, Pallas kernels: none -> 74.7 us  [routed_experts(): pl.pallas_call(routed_kernel, out_shape=jax.ShapeDtypeStruct((spn, cap, w...]
    all_to_all x1 -> x0, blocking collectives: 52.9 us -> none  [per_device(): lax.all_to_all(outgoing, ('sp', 'tp'), split_axis=0, concat_axis=0, tiled...]
    all_to_all x1 -> x0, waiting for transfers between devices: 46 us -> none  [per_device(): lax.all_to_all(produced, ('sp', 'tp'), split_axis=0, concat_axis=0, tiled...]
    gather x1 -> x0, local copies, waits for them, and re-layouts: 5.2 us -> none  [per_device(): picked = returned[position].reshape(row_count, 2, width)]
    all_to_all x1 -> x0, starting transfers between devices: 4.65 us -> none  [per_device(): lax.all_to_all(produced, ('sp', 'tp'), split_axis=0, concat_axis=0, tiled...]
    dot_general x2, matrix products: 8.5 us -> 3.88 us  [the longest x1 2.37 us: route_by_group(): lax.dot_general(pick, back.reshape(spn * cap, width), (((0,), (0,)), ((),...]
    scatter x1 -> x0, local copies, waits for them, and re-layouts: 4.43 us -> none  [per_device(): outgoing = jnp.zeros((experts * capacity, width), jnp.bfloat16).at[positi...]
    reduce_sum x2 -> x3, other arithmetic: 4.91 us -> 0.52 us  [the longest x1 0.34 us: route_by_group(): jnp.sum(jnp.where(chosen[None, :, :], by_expert.T[:, None, :], 0.0), axis=2)]
  transfers between devices with their start and end apart: 3 -> 2, of which waited for: 2 -> 1; matrix products, arithmetic and copies ran while one was open for 3% -> 5% of each run, Pallas kernels for 0% -> 0%
where the time goes in v1:
time: 119 us
  Pallas kernels  74.7 us (63%)
  other arithmetic  12.4 us (10%)
  blocking collectives  12.3 us (10%)
  starting transfers between devices  7.54 us (6%)
  matrix products  6.88 us (6%)
  waiting for transfers between devices  3.99 us (3%)
    pallas_call x1, Pallas kernels, routed_experts(): pl.pallas_call(routed_kernel, out_shape=jax.ShapeDtypeStruct((spn, cap, w...  74.7 us
    psum x1, blocking collectives, per_device(): energy = lax.psum(jnp.sum(swished * swished, axis=1), 'tp')  6.31 us
    psum x1, blocking collectives, per_device(): lax.psum((jnp.sum(convolved, axis=1), jnp.sum(convolved * convolved, axis...  5.97 us
    all_to_all x1, starting transfers between devices, per_device(): lax.all_to_all(branch, 'tp', split_axis=0, concat_axis=1, tiled=True)  4.34 us
    all_to_all x1, waiting for transfers between devices, per_device(): lax.all_to_all(branch, 'tp', split_axis=0, concat_axis=1, tiled=True)  3.99 us
    reduce_sum x1, other arithmetic, per_device(): jnp.sum(convolved, axis=1)  3.23 us
    ppermute x1, starting transfers between devices, passed_along(): return lax.ppermute(block, axis, route)  3.2 us
    dot_general x1, matrix products, per_device(): jnp.dot(regrouped, out_weight, preferred_element_type=jnp.float32)  3.01 us
  transfers between devices with their start and end apart: 2, of which 1 were waited for; matrix products, arithmetic and copies ran while one was open for 5% of the time, Pallas kernels for 0%

profile of v1, /device:TPU:13, one launch (start us, length us, event | category | flops | bytes accessed | tf_op | source)
XLA Modules:
  0.0 118.8 jit_solution(8927547044767385916)
XLA Ops:
  0.0 1.2 %multiply_convert_fusion.3 = bf16[512,256]{1,0:T(8,128)(2,1)S(1)} fusion(bf16[512,256]{1,0:T(8,128)(2,1)} %param.16, bf16[512,256]{1,0:T(8,128)(2,1)} %param.15), kind=kLoop, calls=%fused_computation.45 | loop fusion | flops 917504 | bytes 786432 | tf_op jit(solution)/shard_map/convert_element_type | solution.py:264
  1.3 3.2 %collective-permute-start = (bf16[30,256]{1,0:T(8,128)(2,1)S(1)}, bf16[30,256]{1,0:T(8,128)(2,1)S(1)}, u32[]{:S(2)}, u32[]{:S(2)}) collective-permute-start(bf16[30,256]{1,0:T(8,128)(2,1)S(1)} %slice.252), channel_id=1, source_target_pairs={{0,4},{4,8},{8,12},{1,5},{5,9},{9,13},{2,6},{6,10},{10,14},{3,7},{... | collective-permute-start | bytes 46088 | tf_op jit(solution)/shard_map/ppermute | solution.py:241
  4.5 0.7 fusion.42
  5.2 0.7 and_select_fusion.5
  5.9 1.0 slice_convert_fusion.29
  6.8 1.0 slice_convert_fusion.30
  7.9 0.2 convert_reduce_fusion
  8.0 0.7 multiply_add_fusion.1
  8.8 0.7 and_select_fusion
  9.5 3.2 %fusion.43 = (f32[512]{0:T(512)S(1)}, f32[512]{0:T(512)S(1)}, f32[512,256]{1,0:T(8,128)S(1)}) fusion(f32[256]{0:T(256)S(1)} %bitcast.77, bf16[512,256]{1,0:T(8,128)(2,1)S(1)} %multiply_convert_fusion.3, f32[256]{0:T(256)S(1)} %bitcast.78, bf16[30,256]{1,0:T(8,128)(2,1)S(1)} %collective-permute-done, f32[256]{0:T(256)S(1)} %bitcast.80, f32[256]{0:T(256)S(1)} %bitcast.81, ...), kind=kLoop, calls=%fused_computation.154 | loop fusion | flops 24378368 | bytes 838656 | tf_op jit(solution)/shard_map/reduce_sum | solution.py:274
  12.7 6.0 %all-reduce.1 = (f32[512]{0:T(512)S(1)}, f32[512]{0:T(512)S(1)}) all-reduce(f32[512]{0:T(512)S(1)} %get-tuple-element.6, f32[512]{0:T(512)S(1)} %get-tuple-element.5), channel_id=1, replica_groups=mesh['grp'=2,'sp'=4,'tp'=4] {'tp'}, use_global_device_ids=true, to_apply=%region_3.0 | all-reduce | flops 1024 | bytes 8192 | tf_op jit(solution)/shard_map/psum | solution.py:274
  18.7 1.0 multiply_reduce_fusion.1
  19.8 6.3 %psum.23 = f32[512]{0:T(512)S(1)} all-reduce(f32[512]{0:T(512)S(1)} %get-tuple-element.9), channel_id=1, replica_groups=mesh['grp'=2,'sp'=4,'tp'=4] {'tp'}, use_global_device_ids=true, to_apply=%region_5.6 | all-reduce | flops 512 | bytes 4096 | tf_op jit(solution)/shard_map/psum | solution.py:278
  26.1 1.5 %multiply_convert_fusion.2 = bf16[512,256]{1,0:T(8,128)(2,1)} fusion(f32[512,256]{1,0:T(8,128)S(1)} %get-tuple-element.10, f32[256]{0:T(256)} %param.21, f32[512]{0:T(512)S(1)} %add_rsqrt_fusion), kind=kLoop, calls=%fused_computation.40 | loop fusion | flops 393216 | bytes 789504 | tf_op jit(solution)/shard_map/convert_element_type | solution.py:279
  27.6 4.3 %all-to-all-start = ((bf16[4,128,256]{2,1,0:T(8,128)(2,1)}), bf16[4,128,256]{2,1,0:T(8,128)(2,1)S(1)}, u32[]{:S(2)}, u32[]{:S(2)}) async-start(bf16[4,128,256]{2,1,0:T(8,128)(2,1)} %bitcast.31), calls=%async_computation | async-start | bytes 524288 | tf_op jit(solution)/shard_map/all_to_all | solution.py:283
  31.9 0.3 select_reduce_fusion
  32.3 0.1 reshape.144
  32.4 0.6 pad.4.meta
  33.0 4.0 %all-to-all-done = bf16[4,128,256]{2,1,0:T(8,128)(2,1)S(1)} async-done(((bf16[4,128,256]{2,1,0:T(8,128)(2,1)}), bf16[4,128,256]{2,1,0:T(8,128)(2,1)S(1)}, u32[]{:S(2)}, u32[]{:S(2)}) %all-to-all-start) | async-done | bytes 262176 | tf_op jit(solution)/shard_map/all_to_all | solution.py:283
  37.0 0.2 copy.25
  37.2 3.0 %multiply_reduce_fusion = (f32[128]{0:T(128)S(1)}, f32[128,2048]{1,0:T(8,128)S(1)}) fusion(bf16[128,1024]{0,1:T(8,128)(2,1)S(1)} %bitcast.63, bf16[1024,2048]{1,0:T(8,128)(2,1)} %param.22, bf16[128,2048]{1,0:T(8,128)(2,1)S(1)} %copy-done), kind=kOutput, calls=%fused_computation.37 | convolution fusion | flops 538443648 | bytes 6029824 | tf_op jit(solution)/shard_map/dot_general | solution.py:284
  40.2 1.5 %convolution_convert_fusion = bf16[256,2048]{1,0:T(8,128)(2,1)} fusion(f32[128,2048]{1,0:T(8,128)S(1)} %get-tuple-element.46, f32[2048]{0:T(1024)S(1)} %copy-done.1, f32[128]{0:T(128)S(1)} %add_rsqrt_fusion.2, s32[128]{0:T(128)S(1)} %multiply_add_fusion.1), kind=kOutput, calls=%fused_computation.29 | convolution fusion | flops 135561216 | bytes 2106368 | tf_op jit(solution)/shard_map/dot_general | solution.py:224
  41.7 74.7 %shard_map.145 = bf16[4,64,2048]{2,1,0:T(8,128)(2,1)} custom-call(bf16[4,64,2048]{2,1,0:T(8,128)(2,1)} %bitcast.59, f32[4,8,128]{2,1,0:T(8,128)} %pad.4.meta, bf16[2048,512]{1,0:T(8,128)(2,1)} %bitcast.60, bf16[2048,512]{1,0:T(8,128)(2,1)} %bitcast.61, bf16[512,2048]{1,0:T(8,128)(2,1)} %bitcast.62), custom_call_target="tpu_custom_call" | custom-call | tf_op jit(solution)/shard_map/pallas_call | solution.py:185
  116.4 2.4 %fusion = bf16[128,2048]{1,0:T(8,128)(2,1)} fusion(f32[128,2048]{1,0:T(8,128)S(1)} %get-tuple-element.46, bf16[256,2048]{1,0:T(8,128)(2,1)} %bitcast.58, s32[128]{0:T(128)S(1)} %multiply_add_fusion.1), kind=kOutput, calls=%fused_computation.32 | convolution fusion | flops 134774784 | bytes 2621952 | tf_op jit(solution)/shard_map/dot_general | solution.py:232
  (14 shorter events, 0.1 us)
Async XLA Ops:
  0.0 31.9 %copy-start.2 = (f32[128,2]{0,1:T(2,128)S(1)}, f32[128,2]{0,1:T(2,128)}, u32[]{:S(2)}) copy-start(f32[128,2]{0,1:T(2,128)} %param.26) | copy-start | bytes 3076
  0.0 37.1 %copy-start = (bf16[128,2048]{1,0:T(8,128)(2,1)S(1)}, bf16[128,2048]{1,0:T(8,128)(2,1)}, u32[]{:S(2)}) copy-start(bf16[128,2048]{1,0:T(8,128)(2,1)} %param.23) | copy-start | bytes 1572868
  1.3 8.2 %collective-permute-start = (bf16[30,256]{1,0:T(8,128)(2,1)S(1)}, bf16[30,256]{1,0:T(8,128)(2,1)S(1)}, u32[]{:S(2)}, u32[]{:S(2)}) collective-permute-start(bf16[30,256]{1,0:T(8,128)(2,1)S(1)} %slice.252), channel_id=1, source_target_pairs={{0,4},{4,8},{8,12},{1,5},{5,9},{9,13},{2,6},{6,10},{10,14},{3,7},{... | collective-permute-start | bytes 46088 | tf_op jit(solution)/shard_map/ppermute | solution.py:241
  19.7 20.4 %copy-start.1 = (f32[2048]{0:T(1024)S(1)}, f32[2048]{0:T(1024)}, u32[]{:S(2)}) copy-start(f32[2048]{0:T(1024)} %param.24) | copy-start | bytes 24580
  27.6 9.4 %all-to-all-start = ((bf16[4,128,256]{2,1,0:T(8,128)(2,1)}), bf16[4,128,256]{2,1,0:T(8,128)(2,1)S(1)}, u32[]{:S(2)}, u32[]{:S(2)}) async-start(bf16[4,128,256]{2,1,0:T(8,128)(2,1)} %bitcast.31), calls=%async_computation | async-start | bytes 524288 | tf_op jit(solution)/shard_map/all_to_all | solution.py:283

commit v2 on v1

--- a/solution.py
+++ b/solution.py
@@ -20,16 +20,25 @@
     return total
 
 
-def routed_kernel(
-    send, meta, gate_hbm, up_hbm, down_hbm, out,
-    w_gate, w_up, w_down, rows, weights, own, half_out, half_in, cross_out, cross_in, final, act,
-    load_sem, meta_s, meta_r, z_s, z_r, pair_s, pair_r, x_s, x_r, via_s, via_r,
+def layer_kernel(
+    value, gate, taps, params, residual, moe_gain, meta, pick, unpick,
+    out_hbm, gate_hbm, up_hbm, down_hbm, result,
+    w_out, w_gate, w_up, w_down, padded, conv, wide, gains, branch, hid, send, back,
+    rows, weights, own, half_out, half_in, cross_out, cross_in, final, act,
+    load_sem, meta_s, meta_r, halo_s, halo_r, gain_s, gain_r, group_s, group_r,
+    z_s, z_r, pair_s, pair_r, x_s, x_r, via_s, via_r,
     half_s, half_r, cross_s, cross_r, back_s, back_r,
 ):
     spn, tpn, cap, width = rows.shape
     me_z, me_t = lax.axis_index("sp"), lax.axis_index("tp")
     pair, across = flipped(me_t, 1, tpn), flipped(me_t, 2, tpn)
     hidden = w_gate.shape[1]
+    tok_rows, channels = value.shape
+    row_count = tok_rows // tpn
+    full = channels * tpn
+    reach = padded.shape[0] - tok_rows
+    tap_count = taps.shape[0]
+    f32, bf = jnp.float32, jnp.bfloat16
 
     def to(z, t):
         return {"sp": z, "tp": t}
@@ -41,7 +50,7 @@
 
     loads = [
         pltpu.make_async_copy(a, b, load_sem.at[i])
-        for i, (a, b) in enumerate(((gate_hbm, w_gate), (up_hbm, w_up), (down_hbm, w_down)))
+        for i, (a, b) in enumerate(((out_hbm, w_out), (gate_hbm, w_gate), (up_hbm, w_up), (down_hbm, w_down)))
     ]
     for load in loads:
         load.start()
@@ -52,7 +61,24 @@
         pl.semaphore_signal(
             barrier, inc=1, device_id=to(flipped(me_z, k, spn), flipped(me_t, r, tpn)), device_id_type=MESH
         )
+
+    gated = value[...].astype(f32) / (1.0 + jnp.exp(-gate[...].astype(f32)))
+    padded[reach:, :] = gated.astype(bf).astype(f32)
     pl.semaphore_wait(barrier, len(peers))
+
+    mine = pl.ds(pl.multiple_of(me_t * channels, channels), channels)
+
+    def halo_copy(z):
+        return copy(
+            padded.at[pl.ds(tok_rows, reach)], padded.at[pl.ds(0, reach)], halo_s.at[0], halo_r.at[0], z, me_t
+        )
+
+    def gain_copy(r):
+        return copy(params, gains.at[:, mine], gain_s.at[r], gain_r.at[r], me_z, flipped(me_t, r, tpn))
+
+    def group_copy(r):
+        t = flipped(me_t, r, tpn)
+        return copy(conv.at[t], wide.at[:, mine], group_s.at[r], group_r.at[r], me_z, t)
 
     def z_copy(k):
         return copy(send.at[k], rows.at[k, 0], z_s.at[k], z_r.at[k], flipped(me_z, k, spn), me_t)
@@ -79,22 +105,95 @@
         return copy(cross_out.at[k], cross_in.at[k], cross_s.at[k], cross_r.at[k], me_z, across)
 
     def back_copy(k):
-        return copy(final.at[k], out.at[k], back_s.at[k], back_r.at[k], flipped(me_z, k, spn), me_t)
-
+        return copy(final.at[k], back.at[k], back_s.at[k], back_r.at[k], flipped(me_z, k, spn), me_t)
+
+    @pl.when(me_z < spn - 1)
+    def _():
+        halo_copy(me_z + 1).start()
+
+    for r in range(1, tpn):
+        gain_copy(r).start()
     for k, r in peers:
         meta_copy(k, r).start()
+    weights[0, 0] = meta[0]
+    gains[:, mine] = params[...]
+
+    piece = min(row_count, 64)
+
+    def convolve(first):
+        total = jnp.zeros((piece, channels), f32) + params[3:4, :]
+        for k in range(tap_count):
+            start = first + reach - tap_count + 1 + k
+            total = total + padded[start : start + piece, :] * taps[k : k + 1, :]
+        block, inner = first // row_count, first % row_count
+        conv[block, inner : inner + piece, :] = total.astype(bf)
+
+    for first in range(piece, tok_rows, piece):
+        convolve(first)
+
+    @pl.when(me_z == 0)
+    def _():
+        padded[:reach, :] = jnp.zeros((reach, channels), f32)
+
+    @pl.when(me_z > 0)
+    def _():
+        halo_copy(me_z - 1).wait_recv()
+
+    convolve(0)
+    for r in range(1, tpn):
+        group_copy(r).start()
+    wide[:, mine] = conv[me_t]
+    for r in range(1, tpn):
+        gain_copy(r).wait_recv()
+    for r in range(1, tpn):
+        group_copy(r).wait_recv()
+
+    part = min(row_count, 32)
+    for first in range(0, row_count, part):
+        v = wide[first : first + part, :].astype(f32)
+        average = jnp.sum(v, axis=1, keepdims=True) / full
+        spread = jnp.sum(v * v, axis=1, keepdims=True) / full - average * average
+        v = (v - average) * lax.rsqrt(spread + EPSILON) * gains[0:1, :] + gains[1:2, :]
+        v = v / (1.0 + jnp.exp(-v))
+        energy = jnp.sum(v * v, axis=1, keepdims=True) / full
+        branch[first : first + part, :] = (v * lax.rsqrt(energy + EPSILON) * gains[2:3, :]).astype(bf)
+
+    tile = min(hidden, 512)
+    loads[0].wait()
+
+    def project(c, power):
+        cols = pl.ds(pl.multiple_of(c * tile, tile), tile)
+        h = residual[:, cols].astype(f32) + jnp.dot(
+            branch[...], w_out[:, cols], preferred_element_type=f32
+        )
+        h = h.astype(bf)
+        hid[:, cols] = h
+        h = h.astype(f32)
+        return power + jnp.sum(h * h, axis=1, keepdims=True)
+
+    power = lax.fori_loop(0, width // tile, project, jnp.zeros((row_count, 1), f32))
+    level = lax.rsqrt(power / width + EPSILON)
+
+    def dispatch(c, carry):
+        cols = pl.ds(pl.multiple_of(c * tile, tile), tile)
+        n = (hid[:, cols].astype(f32) * level * moe_gain[:, cols]).astype(bf)
+        picked = jnp.dot(pick[...], n, preferred_element_type=f32).astype(bf)
+        for k in range(spn):
+            send[k, :, cols] = picked[k * cap : (k + 1) * cap]
+        return carry
+
+    lax.fori_loop(0, width // tile, dispatch, 0)
+
     for k in range(1, spn):
         z_copy(k).start()
-    weights[0, 0] = meta[0]
     rows[0, 0] = send[0]
     x_copy(0).start()
     pair_copy(0).start()
     for k, r in peers:
         meta_copy(k, r).wait_recv()
-    for load in loads:
+    for load in loads[1:]:
         load.wait()
 
-    tile = min(hidden, 512)
     diagonal = (
         lax.broadcasted_iota(jnp.int32, (cap, LANES), 0) == lax.broadcasted_iota(jnp.int32, (cap, LANES), 1)
     )
@@ -163,7 +262,27 @@
         return carry
 
     lax.fori_loop(0, spn + 2, step, 0)
-    out[0] = final[0]
+    back[0] = final[0]
+    for k in range(1, spn):
+        back_copy(k).wait_recv()
+
+    def combine(c, carry):
+        cols = pl.ds(pl.multiple_of(c * tile, tile), tile)
+        total = hid[:, cols].astype(f32)
+        moved = back[:, :, cols].reshape(spn * cap, tile)
+        total = total + jnp.dot(unpick[...], moved, preferred_element_type=f32)
+        result[:, cols] = total.astype(bf)
+        return carry
+
+    lax.fori_loop(0, width // tile, combine, 0)
+
+    @pl.when(me_z < spn - 1)
+    def _():
+        halo_copy(me_z + 1).wait_send()
+
+    for r in range(1, tpn):
+        gain_copy(r).wait_send()
+        group_copy(r).wait_send()
     for k, r in peers:
         meta_copy(k, r).wait_send()
     for k in range(spn):
@@ -172,25 +291,38 @@
     for k in range(1, spn):
         z_copy(k).wait_send()
         back_copy(k).wait_send()
-        back_copy(k).wait_recv()
-
-
-def routed_experts(send, meta, w_gate, w_up, w_down):
-    spn, cap, width = send.shape
-    tpn = lax.axis_size("tp")
+
+
+def whole_layer(
+    value, gate, taps, params, residual, moe_gain, meta, pick, unpick, w_out, w_gate, w_up, w_down
+):
+    spn, tpn = lax.axis_size("sp"), lax.axis_size("tp")
+    cap = pick.shape[0] // spn
+    tok_rows, channels = value.shape
+    row_count, width = residual.shape
     hidden = w_gate.shape[1]
+    reach = -(-(taps.shape[0] - 1) // SUBLANES) * SUBLANES
     bf, f32, dma = jnp.bfloat16, jnp.float32, pltpu.SemaphoreType.DMA
     vmem = pl.BlockSpec(memory_space=pltpu.VMEM)
     hbm = pl.BlockSpec(memory_space=pl.ANY)
     return pl.pallas_call(
-        routed_kernel,
-        out_shape=jax.ShapeDtypeStruct((spn, cap, width), bf),
-        in_specs=[vmem, vmem, hbm, hbm, hbm],
+        layer_kernel,
+        out_shape=jax.ShapeDtypeStruct((row_count, width), bf),
+        in_specs=[vmem] * 9 + [hbm] * 4,
         out_specs=vmem,
         scratch_shapes=[
+            pltpu.VMEM(w_out.shape, bf),
             pltpu.VMEM(w_gate.shape, bf),
             pltpu.VMEM(w_up.shape, bf),
             pltpu.VMEM(w_down.shape, bf),
+            pltpu.VMEM((reach + tok_rows, channels), f32),
+            pltpu.VMEM((tpn, row_count, channels), bf),
+            pltpu.VMEM((row_count, channels * tpn), bf),
+            pltpu.VMEM((SUBLANES, channels * tpn), f32),
+            pltpu.VMEM((row_count, channels * tpn), bf),
+            pltpu.VMEM((row_count, width), bf),
+            pltpu.VMEM((spn, cap, width), bf),
+            pltpu.VMEM((spn, cap, width), bf),
             pltpu.VMEM((spn, tpn, cap, width), bf),
             pltpu.VMEM((spn, tpn, SUBLANES, LANES), f32),
             pltpu.VMEM((spn, 2, cap, width), f32),
@@ -200,18 +332,37 @@
             pltpu.VMEM((spn, cap, width), bf),
             pltpu.VMEM((spn, cap, width), bf),
             pltpu.VMEM((tpn * cap, hidden), bf),
-            dma((3,)),
+            dma((4,)),
             dma((spn, tpn)),
             dma((spn, tpn)),
+            dma((1,)),
+            dma((1,)),
         ]
+        + [dma((tpn,))] * 4
         + [dma((spn,))] * 14,
         compiler_params=pltpu.CompilerParams(collective_id=0, has_side_effects=True),
-    )(send, meta, w_gate, w_up, w_down)
-
-
-def route_by_group(normed, widened, expert_ids, expert_weights, w_gate, w_up, w_down):
+    )(value, gate, taps, params, residual, moe_gain, meta, pick, unpick, w_out, w_gate, w_up, w_down)
+
+
+def fused_layer(
+    conv_value,
+    conv_gate,
+    kernel,
+    conv_bias,
+    ln_gain,
+    ln_bias,
+    out_gain,
+    out_weight,
+    residual,
+    moe_gain,
+    expert_ids,
+    expert_weights,
+    w_gate,
+    w_up,
+    w_down,
+):
     spn, tpn = lax.axis_size("sp"), lax.axis_size("tp")
-    row_count, width = normed.shape
+    row_count, width = residual.shape
     capacity = 2 * row_count // min(row_count, spn * tpn // 2)
     cap = tpn * capacity // 2
     group = expert_ids[:, 0] // tpn
@@ -221,18 +372,19 @@
     slot = flipped(group, lax.axis_index("sp"), spn) * cap + rank
     chosen = jnp.arange(spn * cap, dtype=jnp.int32)[:, None] == slot[None, :]
     pick = chosen.astype(jnp.bfloat16)
-    send = jnp.dot(pick, normed, preferred_element_type=jnp.float32).astype(jnp.bfloat16)
     member = (expert_ids[:, :, None] % tpn) == jnp.arange(SUBLANES, dtype=jnp.int32)[None, None, :]
     by_expert = jnp.sum(jnp.where(member, expert_weights[:, :, None], 0.0), axis=1)
     meta = jnp.sum(
         jnp.where(chosen[None, :, :], by_expert.T[:, None, :], 0.0), axis=2
     ).reshape(SUBLANES, spn, cap)
     meta = jnp.pad(meta.transpose(1, 0, 2), ((0, 0), (0, 0), (0, LANES - cap)))
-    back = routed_experts(send.reshape(spn, cap, width), meta, w_gate[0], w_up[0], w_down[0])
-    combined = lax.dot_general(
-        pick, back.reshape(spn * cap, width), (((0,), (0,)), ((), ())), preferred_element_type=jnp.float32
-    )
-    return (widened + combined).astype(jnp.bfloat16)
+    unpick = (slot[:, None] == jnp.arange(spn * cap, dtype=jnp.int32)[None, :]).astype(jnp.bfloat16)
+    params = jnp.stack([ln_gain, ln_bias, out_gain, conv_bias])
+    params = jnp.pad(params, ((0, SUBLANES - params.shape[0]), (0, 0)))
+    return whole_layer(
+        conv_value, conv_gate, kernel.astype(jnp.float32), params, residual, moe_gain[None, :],
+        meta, pick, unpick, out_weight, w_gate[0], w_up[0], w_down[0],
+    )
 
 
 def passed_along(block, axis, distance):
@@ -258,6 +410,12 @@
     w_up,
     w_down,
 ):
+    tpn = lax.axis_size("tp")
+    if lax.axis_size("sp") == GROUPS and tpn == 4:
+        return fused_layer(
+            conv_value, conv_gate, kernel, conv_bias, ln_gain, ln_bias, out_gain, out_weight, residual,
+            moe_gain, expert_ids, expert_weights, w_gate, w_up, w_down,
+        )
     tok_rows, channels = conv_value.shape
     reach_rows = kernel.shape[0] - 1
     full_channels = channels * lax.axis_size("tp")
@@ -289,10 +447,6 @@
     ).astype(jnp.bfloat16)
     width = normed.shape[1]
     experts = lax.axis_size("sp") * lax.axis_size("tp")
-    if experts // GROUPS == lax.axis_size("tp") and lax.axis_size("tp") == 4:
-        return route_by_group(
-            normed, widened, expert_ids, expert_weights, w_gate, w_up, w_down
-        )
     capacity = 2 * row_count // min(row_count, experts // 2)
     flat_ids = expert_ids.reshape(-1)
     onehot = (flat_ids[:, None] == jnp.arange(experts, dtype=jnp.int32)[None, :]).astype(jnp.int32)

time: 119 us -> 98.4 us (0.83)
  blocking collectives: 12.3 us -> 0 us
  Pallas kernels: 74.7 us -> 86.8 us
  starting transfers between devices: 7.54 us -> 0 us
  matrix products: 6.88 us -> 0 us
  waiting for transfers between devices: 3.99 us -> 0 us
  other arithmetic: 12.4 us -> 8.7 us
  local copies, waits for them, and re-layouts: 0.88 us -> 2.57 us
    psum x2 -> x0, blocking collectives: 12.3 us -> none  [the longest x1 6.31 us: per_device(): energy = lax.psum(jnp.sum(swished * swished, axis=1), 'tp')]
    pallas_call x1, Pallas kernels: 74.7 us -> 86.8 us  [whole_layer(): pl.pallas_call(layer_kernel, out_shape=jax.ShapeDtypeStruct((row_count, w...]
    dot_general x3 -> x0, matrix products: 6.88 us -> none  [the longest x1 3.01 us: per_device(): jnp.dot(regrouped, out_weight, preferred_element_type=jnp.float32)]
    all_to_all x1 -> x0, starting transfers between devices: 4.34 us -> none  [per_device(): lax.all_to_all(branch, 'tp', split_axis=0, concat_axis=1, tiled=True)]
    all_to_all x1 -> x0, waiting for transfers between devices: 3.99 us -> none  [per_device(): lax.all_to_all(branch, 'tp', split_axis=0, concat_axis=1, tiled=True)]
    reduce_sum x5 -> x3, other arithmetic: 4.8 us -> 1.2 us  [the longest x1 0.69 us: fused_layer(): jnp.sum(jnp.where(member, expert_weights[:, :, None], 0.0), axis=1)]
    ppermute x1 -> x0, starting transfers between devices: 3.2 us -> none  [passed_along(): return lax.ppermute(block, axis, route)]
    mul x2 -> x0, other arithmetic: 1.97 us -> none  [per_device(): padded[offset:offset + tok_rows].astype(jnp.float32)]
  transfers between devices with their start and end apart: 2 -> 0, of which waited for: 1 -> 0; matrix products, arithmetic and copies ran while one was open for 5% -> 0% of each run, Pallas kernels for 0% -> 0%
where the time goes in v2:
time: 98.4 us; the launch traced here: 98.1 us
  Pallas kernels  86.8 us (88%)
  other arithmetic  8.7 us (9%)
  local copies, waits for them, and re-layouts  2.57 us (3%)
    pallas_call x1, Pallas kernels, whole_layer(): pl.pallas_call(layer_kernel, out_shape=jax.ShapeDtypeStruct((row_count, w...  86.8 us

profile of v2, /device:TPU:13, one launch (start us, length us, event | category | flops | bytes accessed | tf_op | source)
XLA Modules:
  0.0 98.1 jit_solution(9469884601901294862)
XLA Ops:
  0.0 0.7 fusion.13
  0.7 0.7 and_select_fusion.8
  1.4 0.2 convert_reduce_fusion
  1.5 0.7 fusion.12
  2.3 0.7 multiply_add_fusion
  3.0 0.7 and_select_fusion.3
  3.7 0.7 select_reduce_fusion.1
  4.3 1.3 %select_maximum_fusion.params = f32[8,256]{1,0:T(8,128)} fusion(f32[1,256]{1,0:T(1,128)} %bitcast.36, f32[1,256]{1,0:T(1,128)} %bitcast.37, f32[1,256]{1,0:T(1,128)} %bitcast.38, f32[1,256]{1,0:T(1,128)} %bitcast.39), kind=kLoop, calls=%fused_computation.8 | loop fusion | flops 16384 | bytes 12288 | tf_op jit(solution)/shard_map/stack | solution.py:382
  5.7 1.3 %convert_element_type.16.taps = f32[31,256]{1,0:T(8,128)} convert(bf16[31,256]{1,0:T(8,128)(2,1)} %param.17) | non-fusion elementwise | flops 7936 | bytes 47616 | tf_op jit(solution)/shard_map/convert_element_type | solution.py:385
  7.0 0.7 fusion.unpick
  7.7 0.7 fusion.2
  8.4 0.3 select_reduce_fusion
  8.7 0.1 reshape.115
  8.8 0.6 pad.9.meta
  9.4 86.8 %shard_map.145 = bf16[128,2048]{1,0:T(8,128)(2,1)} custom-call(bf16[512,256]{1,0:T(8,128)(2,1)} %value.1, bf16[512,256]{1,0:T(8,128)(2,1)} %gate.1, f32[31,256]{1,0:T(8,128)} %convert_element_type.16.taps, f32[8,256]{1,0:T(8,128)} %select_maximum_fusion.params, bf16[128,2048]{1,0:T(8,128)(2,1)} %residual.1, f32[1,2048]{1,0:T(1,128)} %bitcast.35, ...), custom_call_target="tpu_custom_call" | custom-call | tf_op jit(solution)/shard_map/pallas_call | solution.py:308
  96.2 1.9 %copy.25 = bf16[128,2048]{1,0:T(8,128)(2,1)} copy(bf16[128,2048]{1,0:T(8,128)(2,1)} %shard_map.145) | data formatting | bytes 1048576
  (1 shorter events, 0.0 us)

commit v3 on v2

--- a/solution.py
+++ b/solution.py
@@ -7,6 +7,7 @@
 
 EPSILON = 1e-06
 GROUPS = 4
+SPLIT = 2
 LANES = 128
 SUBLANES = 8
 MESH = pl.DeviceIdType.MESH
@@ -21,15 +22,17 @@
 
 
 def layer_kernel(
-    value, gate, taps, params, residual, moe_gain, meta, pick, unpick,
+    value, gate, kernel, conv_bias, ln_gain, ln_bias, out_gain, residual, moe_gain, ids, shares,
     out_hbm, gate_hbm, up_hbm, down_hbm, result,
-    w_out, w_gate, w_up, w_down, padded, conv, wide, gains, branch, hid, send, back,
+    w_out, w_gate, w_up, w_down, taps, params, meta, pick, unpick, padded, conv, wide, gains, branch, hid, send, back,
     rows, weights, own, half_out, half_in, cross_out, cross_in, final, act,
     load_sem, meta_s, meta_r, halo_s, halo_r, gain_s, gain_r, group_s, group_r,
     z_s, z_r, pair_s, pair_r, x_s, x_r, via_s, via_r,
     half_s, half_r, cross_s, cross_r, back_s, back_r,
 ):
-    spn, tpn, cap, width = rows.shape
+    spn, tpn = weights.shape[:2]
+    pieces, _, height, width = rows.shape
+    cap = height * SPLIT
     me_z, me_t = lax.axis_index("sp"), lax.axis_index("tp")
     pair, across = flipped(me_t, 1, tpn), flipped(me_t, 2, tpn)
     hidden = w_gate.shape[1]
@@ -37,7 +40,7 @@
     row_count = tok_rows // tpn
     full = channels * tpn
     reach = padded.shape[0] - tok_rows
-    tap_count = taps.shape[0]
+    tap_count = kernel.shape[0]
     f32, bf = jnp.float32, jnp.bfloat16
 
     def to(z, t):
@@ -62,6 +65,38 @@
             barrier, inc=1, device_id=to(flipped(me_z, k, spn), flipped(me_t, r, tpn)), device_id_type=MESH
         )
 
+    params[...] = jnp.zeros_like(params)
+    for i, given in enumerate((ln_gain, ln_bias, out_gain, conv_bias)):
+        params[i : i + 1, :] = given[...]
+    taps[:tap_count, :] = kernel[...].astype(f32)
+
+    square = (row_count, row_count)
+    down, along = (lax.broadcasted_iota(jnp.int32, square, d) for d in (0, 1))
+    group = jnp.broadcast_to(lax.div(ids[:, 0:1], tpn), square)
+    group_row = jnp.broadcast_to(
+        jnp.sum(jnp.where(down == along, group, 0), axis=0, keepdims=True), square
+    )
+    same = group == group_row
+    rank = jnp.sum(jnp.where(same & (along < down), 1, 0), axis=1, keepdims=True)
+    rank_row = jnp.sum(jnp.where(same & (down < along), 1, 0), axis=0, keepdims=True)
+    slot = jnp.bitwise_xor(group[:, 0:1], me_z) * cap + rank
+    slot_row = jnp.bitwise_xor(group_row[0:1, :], me_z) * cap + rank_row
+    slots = spn * cap
+    pick[...] = jnp.where(
+        lax.broadcasted_iota(jnp.int32, (slots, row_count), 0) == slot_row, 1.0, 0.0
+    ).astype(bf)
+    unpick[...] = jnp.where(
+        lax.broadcasted_iota(jnp.int32, (row_count, slots), 1) == slot, 1.0, 0.0
+    ).astype(bf)
+    lane = lax.broadcasted_iota(jnp.int32, (row_count, LANES), 1)
+    expert = lax.rem(ids[...], tpn)
+    meta[...] = jnp.zeros_like(meta)
+    for k in range(spn):
+        here = (lane + k * cap == slot) & (lane < cap)
+        for e in range(tpn):
+            share = jnp.sum(jnp.where(expert == e, shares[...], 0.0), axis=1, keepdims=True)
+            meta[k, e : e + 1, :] = jnp.sum(jnp.where(here, share, 0.0), axis=0, keepdims=True)
+
     gated = value[...].astype(f32) / (1.0 + jnp.exp(-gate[...].astype(f32)))
     padded[reach:, :] = gated.astype(bf).astype(f32)
     pl.semaphore_wait(barrier, len(peers))
@@ -81,7 +116,7 @@
         return copy(conv.at[t], wide.at[:, mine], group_s.at[r], group_r.at[r], me_z, t)
 
     def z_copy(k):
-        return copy(send.at[k], rows.at[k, 0], z_s.at[k], z_r.at[k], flipped(me_z, k, spn), me_t)
+        return copy(send.at[k], rows.at[k, 0], z_s.at[k], z_r.at[k], flipped(me_z, k // SPLIT, spn), me_t)
 
     def meta_copy(k, r):
         return copy(
@@ -105,7 +140,7 @@
         return copy(cross_out.at[k], cross_in.at[k], cross_s.at[k], cross_r.at[k], me_z, across)
 
     def back_copy(k):
-        return copy(final.at[k], back.at[k], back_s.at[k], back_r.at[k], flipped(me_z, k, spn), me_t)
+        return copy(final.at[k], back.at[k], back_s.at[k], back_r.at[k], flipped(me_z, k // SPLIT, spn), me_t)
 
     @pl.when(me_z < spn - 1)
     def _():
@@ -178,15 +213,16 @@
         cols = pl.ds(pl.multiple_of(c * tile, tile), tile)
         n = (hid[:, cols].astype(f32) * level * moe_gain[:, cols]).astype(bf)
         picked = jnp.dot(pick[...], n, preferred_element_type=f32).astype(bf)
-        for k in range(spn):
-            send[k, :, cols] = picked[k * cap : (k + 1) * cap]
+        for k in range(pieces):
+            send[k, :, cols] = picked[k * height : (k + 1) * height]
         return carry
 
     lax.fori_loop(0, width // tile, dispatch, 0)
 
-    for k in range(1, spn):
+    for k in range(SPLIT, pieces):
         z_copy(k).start()
-    rows[0, 0] = send[0]
+    for k in range(SPLIT):
+        rows[k, 0] = send[k]
     x_copy(0).start()
     pair_copy(0).start()
     for k, r in peers:
@@ -194,19 +230,18 @@
     for load in loads[1:]:
         load.wait()
 
-    diagonal = (
-        lax.broadcasted_iota(jnp.int32, (cap, LANES), 0) == lax.broadcasted_iota(jnp.int32, (cap, LANES), 1)
-    )
+    row_of, lane_of = (lax.broadcasted_iota(jnp.int32, (height, LANES), d) for d in (0, 1))
 
     def compute(k):
-        x = rows[k].reshape(tpn * cap, width)
+        x = rows[k].reshape(tpn * height, width)
+        diagonal = lane_of == row_of + (k % SPLIT) * height
         for c in range(0, hidden, 256):
             g = jnp.dot(x, w_gate[:, c : c + 256], preferred_element_type=jnp.float32)
             u = jnp.dot(x, w_up[:, c : c + 256], preferred_element_type=jnp.float32)
             act[:, c : c + 256] = (g / (1.0 + jnp.exp(-g)) * u).astype(jnp.bfloat16)
         a = act[...]
         scales = [
-            jnp.sum(jnp.where(diagonal, weights[k, r, pl.ds(me_t, 1), :], 0.0), axis=1, keepdims=True)
+            jnp.sum(jnp.where(diagonal, weights[k // SPLIT, r, pl.ds(me_t, 1), :], 0.0), axis=1, keepdims=True)
             for r in range(tpn)
         ]
 
@@ -214,7 +249,7 @@
             cols = pl.ds(pl.multiple_of(c * tile, tile), tile)
             res = jnp.dot(a, w_down[:, cols], preferred_element_type=jnp.float32).astype(jnp.bfloat16)
             res = res.astype(jnp.float32)
-            parts = [res[r * cap : (r + 1) * cap] * scales[r] for r in range(tpn)]
+            parts = [res[r * height : (r + 1) * height] * scales[r] for r in range(tpn)]
             half_out[k, 0, :, cols] = parts[1].astype(jnp.bfloat16)
             half_out[k, 1, :, cols] = parts[3].astype(jnp.bfloat16)
             own[k, 0, :, cols] = parts[0]
@@ -224,14 +259,17 @@
         lax.fori_loop(0, width // tile, column, 0)
 
     def step(i, carry):
-        @pl.when(i + 1 < spn)
+        @pl.when((i + 1 >= SPLIT) & (i + 1 < pieces))
+        def _():
+            z_copy(i + 1).wait_recv()
+
+        @pl.when(i + 1 < pieces)
         def _():
             k = i + 1
-            z_copy(k).wait_recv()
             x_copy(k).start()
             pair_copy(k).start()
 
-        @pl.when(i < spn)
+        @pl.when(i < pieces)
         def _():
             x_copy(i).wait_recv()
             via_copy(i).start()
@@ -240,7 +278,7 @@
             compute(i)
             half_copy(i).start()
 
-        @pl.when((i >= 1) & (i <= spn))
+        @pl.when((i >= 1) & (i <= pieces))
         def _():
             k = i - 1
             half_copy(k).wait_recv()
@@ -255,15 +293,16 @@
                 own[k, 0] + half_in[k, 0].astype(jnp.float32) + cross_in[k].astype(jnp.float32)
             ).astype(jnp.bfloat16)
 
-            @pl.when(k >= 1)
+            @pl.when(k >= SPLIT)
             def _():
                 back_copy(k).start()
 
         return carry
 
-    lax.fori_loop(0, spn + 2, step, 0)
-    back[0] = final[0]
-    for k in range(1, spn):
+    lax.fori_loop(0, pieces + 2, step, 0)
+    for k in range(SPLIT):
+        back[k] = final[k]
+    for k in range(SPLIT, pieces):
         back_copy(k).wait_recv()
 
     def combine(c, carry):
@@ -285,63 +324,12 @@
         group_copy(r).wait_send()
     for k, r in peers:
         meta_copy(k, r).wait_send()
-    for k in range(spn):
+    for k in range(pieces):
         for make in (x_copy, pair_copy, via_copy, half_copy, cross_copy):
             make(k).wait_send()
-    for k in range(1, spn):
+    for k in range(SPLIT, pieces):
         z_copy(k).wait_send()
         back_copy(k).wait_send()
-
-
-def whole_layer(
-    value, gate, taps, params, residual, moe_gain, meta, pick, unpick, w_out, w_gate, w_up, w_down
-):
-    spn, tpn = lax.axis_size("sp"), lax.axis_size("tp")
-    cap = pick.shape[0] // spn
-    tok_rows, channels = value.shape
-    row_count, width = residual.shape
-    hidden = w_gate.shape[1]
-    reach = -(-(taps.shape[0] - 1) // SUBLANES) * SUBLANES
-    bf, f32, dma = jnp.bfloat16, jnp.float32, pltpu.SemaphoreType.DMA
-    vmem = pl.BlockSpec(memory_space=pltpu.VMEM)
-    hbm = pl.BlockSpec(memory_space=pl.ANY)
-    return pl.pallas_call(
-        layer_kernel,
-        out_shape=jax.ShapeDtypeStruct((row_count, width), bf),
-        in_specs=[vmem] * 9 + [hbm] * 4,
-        out_specs=vmem,
-        scratch_shapes=[
-            pltpu.VMEM(w_out.shape, bf),
-            pltpu.VMEM(w_gate.shape, bf),
-            pltpu.VMEM(w_up.shape, bf),
-            pltpu.VMEM(w_down.shape, bf),
-            pltpu.VMEM((reach + tok_rows, channels), f32),
-            pltpu.VMEM((tpn, row_count, channels), bf),
-            pltpu.VMEM((row_count, channels * tpn), bf),
-            pltpu.VMEM((SUBLANES, channels * tpn), f32),
-            pltpu.VMEM((row_count, channels * tpn), bf),
-            pltpu.VMEM((row_count, width), bf),
-            pltpu.VMEM((spn, cap, width), bf),
-            pltpu.VMEM((spn, cap, width), bf),
-            pltpu.VMEM((spn, tpn, cap, width), bf),
-            pltpu.VMEM((spn, tpn, SUBLANES, LANES), f32),
-            pltpu.VMEM((spn, 2, cap, width), f32),
-            pltpu.VMEM((spn, 2, cap, width), bf),
-            pltpu.VMEM((spn, 2, cap, width), bf),
-            pltpu.VMEM((spn, cap, width), bf),
-            pltpu.VMEM((spn, cap, width), bf),
-            pltpu.VMEM((spn, cap, width), bf),
-            pltpu.VMEM((tpn * cap, hidden), bf),
-            dma((4,)),
-            dma((spn, tpn)),
-            dma((spn, tpn)),
-            dma((1,)),
-            dma((1,)),
-        ]
-        + [dma((tpn,))] * 4
-        + [dma((spn,))] * 14,
-        compiler_params=pltpu.CompilerParams(collective_id=0, has_side_effects=True),
-    )(value, gate, taps, params, residual, moe_gain, meta, pick, unpick, w_out, w_gate, w_up, w_down)
 
 
 def fused_layer(
@@ -362,28 +350,61 @@
     w_down,
 ):
     spn, tpn = lax.axis_size("sp"), lax.axis_size("tp")
+    tok_rows, channels = conv_value.shape
     row_count, width = residual.shape
+    hidden = w_gate.shape[2]
     capacity = 2 * row_count // min(row_count, spn * tpn // 2)
     cap = tpn * capacity // 2
-    group = expert_ids[:, 0] // tpn
-    place = jnp.arange(row_count, dtype=jnp.int32)
-    earlier = (group[None, :] == group[:, None]) & (place[None, :] < place[:, None])
-    rank = jnp.sum(earlier.astype(jnp.int32), axis=1)
-    slot = flipped(group, lax.axis_index("sp"), spn) * cap + rank
-    chosen = jnp.arange(spn * cap, dtype=jnp.int32)[:, None] == slot[None, :]
-    pick = chosen.astype(jnp.bfloat16)
-    member = (expert_ids[:, :, None] % tpn) == jnp.arange(SUBLANES, dtype=jnp.int32)[None, None, :]
-    by_expert = jnp.sum(jnp.where(member, expert_weights[:, :, None], 0.0), axis=1)
-    meta = jnp.sum(
-        jnp.where(chosen[None, :, :], by_expert.T[:, None, :], 0.0), axis=2
-    ).reshape(SUBLANES, spn, cap)
-    meta = jnp.pad(meta.transpose(1, 0, 2), ((0, 0), (0, 0), (0, LANES - cap)))
-    unpick = (slot[:, None] == jnp.arange(spn * cap, dtype=jnp.int32)[None, :]).astype(jnp.bfloat16)
-    params = jnp.stack([ln_gain, ln_bias, out_gain, conv_bias])
-    params = jnp.pad(params, ((0, SUBLANES - params.shape[0]), (0, 0)))
-    return whole_layer(
-        conv_value, conv_gate, kernel.astype(jnp.float32), params, residual, moe_gain[None, :],
-        meta, pick, unpick, out_weight, w_gate[0], w_up[0], w_down[0],
+    pieces, height = spn * SPLIT, cap // SPLIT
+    reach = -(-(kernel.shape[0] - 1) // SUBLANES) * SUBLANES
+    bf, f32, dma = jnp.bfloat16, jnp.float32, pltpu.SemaphoreType.DMA
+    vmem = pl.BlockSpec(memory_space=pltpu.VMEM)
+    hbm = pl.BlockSpec(memory_space=pl.ANY)
+    return pl.pallas_call(
+        layer_kernel,
+        out_shape=jax.ShapeDtypeStruct((row_count, width), bf),
+        in_specs=[vmem] * 11 + [hbm] * 4,
+        out_specs=vmem,
+        scratch_shapes=[
+            pltpu.VMEM(out_weight.shape, bf),
+            pltpu.VMEM(w_gate.shape[1:], bf),
+            pltpu.VMEM(w_up.shape[1:], bf),
+            pltpu.VMEM(w_down.shape[1:], bf),
+            pltpu.VMEM((reach + SUBLANES, channels), f32),
+            pltpu.VMEM((SUBLANES, channels), f32),
+            pltpu.VMEM((spn, SUBLANES, LANES), f32),
+            pltpu.VMEM((spn * cap, row_count), bf),
+            pltpu.VMEM((row_count, spn * cap), bf),
+            pltpu.VMEM((reach + tok_rows, channels), f32),
+            pltpu.VMEM((tpn, row_count, channels), bf),
+            pltpu.VMEM((row_count, channels * tpn), bf),
+            pltpu.VMEM((SUBLANES, channels * tpn), f32),
+            pltpu.VMEM((row_count, channels * tpn), bf),
+            pltpu.VMEM((row_count, width), bf),
+            pltpu.VMEM((pieces, height, width), bf),
+            pltpu.VMEM((pieces, height, width), bf),
+            pltpu.VMEM((pieces, tpn, height, width), bf),
+            pltpu.VMEM((spn, tpn, SUBLANES, LANES), f32),
+            pltpu.VMEM((pieces, 2, height, width), f32),
+            pltpu.VMEM((pieces, 2, height, width), bf),
+            pltpu.VMEM((pieces, 2, height, width), bf),
+            pltpu.VMEM((pieces, height, width), bf),
+            pltpu.VMEM((pieces, height, width), bf),
+            pltpu.VMEM((pieces, height, width), bf),
+            pltpu.VMEM((tpn * height, hidden), bf),
+            dma((4,)),
+            dma((spn, tpn)),
+            dma((spn, tpn)),
+            dma((1,)),
+            dma((1,)),
+        ]
+        + [dma((tpn,))] * 4
+        + [dma((pieces,))] * 14,
+        compiler_params=pltpu.CompilerParams(collective_id=0, has_side_effects=True),
+    )(
+        conv_value, conv_gate, kernel, conv_bias[None, :], ln_gain[None, :], ln_bias[None, :],
+        out_gain[None, :], residual, moe_gain[None, :], expert_ids, expert_weights,
+        out_weight, w_gate[0], w_up[0], w_down[0],
     )
 
 

time: 98.4 us -> 86.5 us (0.88)
  other arithmetic: 8.7 us -> 0 us
  Pallas kernels: 86.8 us -> 81.5 us
  local copies, waits for them, and re-layouts: 2.57 us -> 4.7 us
    pallas_call x1, Pallas kernels: 86.8 us -> 81.5 us  [fused_layer(): pl.pallas_call(layer_kernel, out_shape=jax.ShapeDtypeStruct((row_count, w...]
    unnamed x1 -> x3, local copies, waits for them, and re-layouts: 1.88 us -> 4.7 us
    convert_element_type x3 -> x0, other arithmetic: 2.69 us -> none  [the longest x1 1.32 us: fused_layer(): kernel.astype(jnp.float32)]
    eq x2 -> x0, other arithmetic: 1.4 us -> none  [the longest x1 0.72 us: fused_layer(): slot[:, None] == jnp.arange(spn * cap, dtype=jnp.int32)[None, :]]
    select_n x2 -> x0, other arithmetic: 1.37 us -> none  [the longest x1 0.69 us: fused_layer(): expert_ids[:, :, None] % tpn]
    another operation x1 -> x0, other arithmetic: 1.33 us -> none  [fused_layer(): params = jnp.stack([ln_gain, ln_bias, out_gain, conv_bias])]
    reduce_sum x3 -> x0, other arithmetic: 1.2 us -> none  [the longest x1 0.69 us: fused_layer(): jnp.sum(jnp.where(member, expert_weights[:, :, None], 0.0), axis=1)]
where the time goes in v3:
time: 86.5 us; the launch traced here: 86.2 us
  Pallas kernels  81.5 us (94%)
  local copies, waits for them, and re-layouts  4.7 us (5%)
    pallas_call x1, Pallas kernels, fused_layer(): pl.pallas_call(layer_kernel, out_shape=jax.ShapeDtypeStruct((row_count, w...  81.5 us
    unnamed x3, local copies, waits for them, and re-layouts  4.7 us

profile of v3, /device:TPU:13, one launch (start us, length us, event | category | flops | bytes accessed | tf_op | source)
XLA Modules:
  0.0 86.2 jit_solution(350816535083498986)
XLA Ops:
  0.0 1.4 %copy.16.ids = s32[128,2]{1,0:T(8,128)} copy(s32[128,2]{0,1:T(2,128)} %param.25) | data formatting | bytes 2048 | tf_op args[10]
  1.4 1.4 %copy.17.shares = f32[128,2]{1,0:T(8,128)} copy(f32[128,2]{0,1:T(2,128)} %param.26) | data formatting | bytes 2048 | tf_op args[11]
  2.8 81.5 %shard_map.145 = bf16[128,2048]{1,0:T(8,128)(2,1)} custom-call(bf16[512,256]{1,0:T(8,128)(2,1)} %value.1, bf16[512,256]{1,0:T(8,128)(2,1)} %gate.1, bf16[31,256]{1,0:T(8,128)(2,1)} %kernel.1, f32[1,256]{1,0:T(1,128)} %bitcast.12, f32[1,256]{1,0:T(1,128)} %bitcast.13, f32[1,256]{1,0:T(1,128)} %bitcast.14, f32[1,256]{1,0:T(1,128)} %bitcast.15, ...), custom_call_target="tpu_custom_call" | custom-call | tf_op jit(solution)/shard_map/pallas_call | solution.py:363
  84.3 1.9 %copy.19 = bf16[128,2048]{1,0:T(8,128)(2,1)} copy(bf16[128,2048]{1,0:T(8,128)(2,1)} %shard_map.145) | data formatting | bytes 1048576

commit v4 on v3

--- a/solution.py
+++ b/solution.py
@@ -72,10 +72,15 @@
 
     square = (row_count, row_count)
     down, along = (lax.broadcasted_iota(jnp.int32, square, d) for d in (0, 1))
-    group = jnp.broadcast_to(lax.div(ids[:, 0:1], tpn), square)
-    group_row = jnp.broadcast_to(
-        jnp.sum(jnp.where(down == along, group, 0), axis=0, keepdims=True), square
-    )
+
+    def upright(line):
+        return jnp.sum(
+            jnp.where(down == along, jnp.broadcast_to(line, square), jnp.zeros((), line.dtype)),
+            axis=1, keepdims=True,
+        )
+
+    group_row = jnp.broadcast_to(lax.div(ids[0:1, :], tpn), square)
+    group = jnp.broadcast_to(upright(group_row[0:1, :]), square)
     same = group == group_row
     rank = jnp.sum(jnp.where(same & (along < down), 1, 0), axis=1, keepdims=True)
     rank_row = jnp.sum(jnp.where(same & (down < along), 1, 0), axis=0, keepdims=True)
@@ -89,12 +94,16 @@
         lax.broadcasted_iota(jnp.int32, (row_count, slots), 1) == slot, 1.0, 0.0
     ).astype(bf)
     lane = lax.broadcasted_iota(jnp.int32, (row_count, LANES), 1)
-    expert = lax.rem(ids[...], tpn)
+    experts = lax.rem(ids[...], tpn)
     meta[...] = jnp.zeros_like(meta)
+    by_expert = [
+        upright(jnp.sum(jnp.where(experts == e, shares[...], 0.0), axis=0, keepdims=True))
+        for e in range(tpn)
+    ]
     for k in range(spn):
         here = (lane + k * cap == slot) & (lane < cap)
         for e in range(tpn):
-            share = jnp.sum(jnp.where(expert == e, shares[...], 0.0), axis=1, keepdims=True)
+            share = by_expert[e]
             meta[k, e : e + 1, :] = jnp.sum(jnp.where(here, share, 0.0), axis=0, keepdims=True)
 
     gated = value[...].astype(f32) / (1.0 + jnp.exp(-gate[...].astype(f32)))
@@ -403,7 +412,7 @@
         compiler_params=pltpu.CompilerParams(collective_id=0, has_side_effects=True),
     )(
         conv_value, conv_gate, kernel, conv_bias[None, :], ln_gain[None, :], ln_bias[None, :],
-        out_gain[None, :], residual, moe_gain[None, :], expert_ids, expert_weights,
+        out_gain[None, :], residual, moe_gain[None, :], expert_ids.T, expert_weights.T,
         out_weight, w_gate[0], w_up[0], w_down[0],
     )
 

time: 86.5 us -> 83.6 us (0.966)
  local copies, waits for them, and re-layouts: 4.7 us -> 1.88 us
    unnamed x3 -> x1, local copies, waits for them, and re-layouts: 4.7 us -> 1.88 us
where the time goes in v4:
time: 83.6 us; the launch traced here: 83.4 us
  Pallas kernels  81.5 us (97%)
  local copies, waits for them, and re-layouts  1.88 us (2%)
    pallas_call x1, Pallas kernels, fused_layer(): pl.pallas_call(layer_kernel, out_shape=jax.ShapeDtypeStruct((row_count, w...  81.5 us
    unnamed x1, local copies, waits for them, and re-layouts  1.88 us

profile of v4, /device:TPU:13, one launch (start us, length us, event | category | flops | bytes accessed | tf_op | source)
XLA Modules:
  0.0 83.4 jit_solution(17244518053644067173)
XLA Ops:
  0.0 81.5 %shard_map.145 = bf16[128,2048]{1,0:T(8,128)(2,1)} custom-call(bf16[512,256]{1,0:T(8,128)(2,1)} %value.1, bf16[512,256]{1,0:T(8,128)(2,1)} %gate.1, bf16[31,256]{1,0:T(8,128)(2,1)} %kernel.1, f32[1,256]{1,0:T(1,128)} %bitcast.14, f32[1,256]{1,0:T(1,128)} %bitcast.15, f32[1,256]{1,0:T(1,128)} %bitcast.16, f32[1,256]{1,0:T(1,128)} %bitcast.17, ...), custom_call_target="tpu_custom_call" | custom-call | tf_op jit(solution)/shard_map/pallas_call | solution.py:372
  81.5 1.9 %copy.17 = bf16[128,2048]{1,0:T(8,128)(2,1)} copy(bf16[128,2048]{1,0:T(8,128)(2,1)} %shard_map.145) | data formatting | bytes 1048576
